TPU v7x, 512 devices: a whole 4x8x8 slice. The times are simulated.
512 devices in a mesh: fs: 64 (over z, y), tp: 8 (over x, core).
Axes of the slice: x: 4, y: 8, z: 8, core: 2. Of those that a mesh axis runs over, the one named last changes fastest.
Arguments:
- tokens: bfloat16 [49152, 2048], P('fs'), may hold values from -6 to 6
- norm_gain: float32 [2048], replicated, may hold values from 0.1 to 1.9
- up_weight: float32 [2048, 8192], P('fs', 'tp'), may hold values from -0.125 to 0.125
- up_scale: float32 [8192], P('tp'), may hold values from 0.5 to 2
- down_weight: float32 [8192, 2048], P('tp', 'fs'), may hold values from -0.1875 to 0.1875
- down_scale: float32 [1, 2048], replicated, may hold values from 0.5 to 2
Outputs:
- mixed: bfloat16 [49152, 2048], P('fs', 'tp')
All inputs are finite; a program needn't handle non-finite values.
Results may differ from a plain program's by a relative error of at most 0.014.
Values may be sent and summed in bfloat16 or wider, within the bound.
A program may use at most 64 MiB of HBM per device.

v0:
```python
import jax
import jax.numpy as jnp
from jax import lax
from jax.sharding import PartitionSpec as P


def on_device(tokens, norm_gain, up_weight, up_scale, down_weight, down_scale):
    values = tokens.astype(jnp.float32)
    normed = (
        values * lax.rsqrt(jnp.mean(values * values, axis=-1, keepdims=True) + 1e-06) * norm_gain
    ).astype(jnp.bfloat16)
    up_cast = up_weight.astype(jnp.bfloat16)
    down_cast = down_weight.astype(jnp.bfloat16)
    up_full = lax.all_gather(up_cast, "fs", axis=0, tiled=True)
    pre = jnp.dot(normed, up_full, preferred_element_type=jnp.float32) * up_scale
    hidden = jnp.square(jnp.maximum(pre, 0.0)).astype(jnp.bfloat16)
    down_full = lax.all_gather(down_cast, "fs", axis=1, tiled=True)
    partial_value = jnp.dot(hidden, down_full, preferred_element_type=jnp.float32) * down_scale
    rounded = partial_value.astype(jnp.bfloat16)
    return (
        lax.psum_scatter(rounded, "tp", scatter_dimension=1, tiled=True)
        .astype(jnp.float32)
        .astype(jnp.bfloat16)
    )


def solution(mesh):
    in_specs = (P("fs", None), P(), P("fs", "tp"), P("tp"), P("tp", "fs"), P())
    out_specs = P("fs", "tp")
    return jax.shard_map(
        on_device, mesh=mesh, in_specs=in_specs, out_specs=out_specs, check_vma=False
    )
```

profile of v0, /device:TPU:1, one launch (start us, length us, event | category | flops | bytes accessed | tf_op | source)
XLA Modules:
  0.0 243.6 jit_solution(16311189245332250504)
XLA Ops:
  6.5 0.0 all-gather.3.cloned.1.call-start
  6.5 1.5 convert_element_type.22
  8.1 0.0 all-gather.3.cloned.1.call-update
  8.1 0.0 all-gather.5.cloned.1.call-start
  8.1 1.5 convert_element_type.24
  9.7 0.0 all-gather.5.cloned.1.call-update
  9.7 0.0 reduce-scatter.2.cloned.1.call-start
  9.8 2.6 %fusion = f32[768]{0:T(1024)S(1)} fusion(bf16[768,2048]{1,0:T(8,128)(2,1)} %param.6), kind=kLoop, calls=%fused_computation.2 | loop fusion | flops 4717824 | bytes 3148800 | tf_op jit(solution)/shard_map/reduce_sum | solution.py:10
  12.3 86.2 %all-gather.3.cloned.1.call-done = bf16[2048,1024]{1,0:T(8,128)(2,1)} async-done(((bf16[32,1024]{1,0:T(8,128)(2,1)}), bf16[2048,1024]{1,0:T(8,128)(2,1)}) %all-gather.3.cloned.1.call-update) | async-done | bytes 4194320 | tf_op jit(solution)/shard_map/all_gather | solution.py:14
  98.6 86.2 %all-gather.5.cloned.1.call-done = bf16[1024,2048]{0,1:T(8,128)(2,1)} async-done(((bf16[1024,32]{0,1:T(8,128)(2,1)}), bf16[1024,2048]{0,1:T(8,128)(2,1)}) %all-gather.5.cloned.1.call-update) | async-done | bytes 4194320 | tf_op jit(solution)/shard_map/all_gather | solution.py:17
  184.8 12.2 %multiply_convert_fusion = bf16[768,2048]{1,0:T(8,128)(2,1)} fusion(bf16[1024,2048]{0,1:T(8,128)(2,1)} %all-gather.5.cloned.1.call-done, f32[2048]{0:T(1024)} %bitcast.3, bf16[2048,1024]{1,0:T(8,128)(2,1)} %all-gather.3.cloned.1.call-done, bf16[768,2048]{1,0:T(8,128)(2,1)} %param.6, f32[2048]{0:T(1024)} %param.7, f32[768]{0:T(1024)S(1)} %add_rsqrt_fusion, ...), kind=kOutput, calls=%fused_computation.5 | convolution fusion | flops 6455033856 | bytes 14703616 | tf_op jit(solution)/shard_map/dot_general | solution.py:18
  197.0 0.0 reduce-scatter.2.cloned.1.call-update
  197.0 40.0 %reduce-scatter.2.cloned.1.call-done = bf16[768,256]{1,0:T(8,128)(2,1)} async-done(((bf16[768,2048]{1,0:T(8,128)(2,1)}), bf16[768,256]{1,0:T(8,128)(2,1)}) %reduce-scatter.2.cloned.1.call-update) | async-done | bytes 393232 | tf_op jit(solution)/shard_map/reduce_scatter | solution.py:21
  (1 shorter events, 0.0 us)
Async XLA Ops:
  6.5 92.0 %all-gather.3.cloned.1.call-start = ((), (), s32[]{:S(2)}) async-start(), calls=%async_computation.1 | async-start | bytes 4259840 | tf_op jit(solution)/shard_map/all_gather | solution.py:14
  8.1 176.7 %all-gather.5.cloned.1.call-start = ((), (), s32[]{:S(2)}) async-start(), calls=%async_computation.2 | async-start | bytes 4259840 | tf_op jit(solution)/shard_map/all_gather | solution.py:17
  9.7 227.3 %reduce-scatter.2.cloned.1.call-start = ((), (), s32[]{:S(2)}) async-start(), calls=%async_computation.3 | async-start | bytes 3538944 | tf_op jit(solution)/shard_map/reduce_scatter | solution.py:21
Sparse Core Ops, SparseCore 0:
  10.4 88.1 all-gather.2
  101.6 83.1 all-gather.4
  197.1 39.8 reduce-scatter.1
where the time goes:
time: 245 us; the launch traced here: 244 us
  waiting for transfers between devices  213 us (87%)
  between operations  13.1 us (5%)
  matrix products  12.2 us (5%)
  other arithmetic  5.65 us (2%)
    all_gather x1, waiting for transfers between devices, on_device(): down_full = lax.all_gather(down_cast, 'fs', axis=1, tiled=True)  86.2 us
    all_gather x1, waiting for transfers between devices, on_device(): up_full = lax.all_gather(up_cast, 'fs', axis=0, tiled=True)  86.2 us
    reduce_scatter x1, waiting for transfers between devices, on_device(): lax.psum_scatter(rounded, 'tp', scatter_dimension=1, tiled=True)  40 us
    dot_general x1, matrix products, on_device(): jnp.dot(hidden, down_full, preferred_element_type=jnp.float32) * down_scale  12.2 us
  transfers between devices with their start and end apart: 3, of which 3 were waited for; matrix products, arithmetic and copies ran while one was open for 2% of the time, Pallas kernels for 0%

commit v1 on v0

v1 whole, which is shorter than its diff:
```python
import functools
import heapq

import jax
import jax.numpy as jnp
from jax import lax
from jax.experimental import pallas as pl
from jax.experimental.pallas import tpu as pltpu
from jax.sharding import PartitionSpec as P

MESH = pl.DeviceIdType.MESH
R = 8
COLS = (0, 1, -1, 2, -2, 3, -3, 4)
ROWS = 16
WIRE, HOP, DEPTH = 0.703, 2.0, 3


def limits(t):
    return (4, 3) if t == 0 else (3, 4)


def col_rank(d):
    return COLS.index(4 if d == -4 else d)


def build_messages():
    msgs = {}
    for t in (0, 1):
        plus, minus = limits(t)
        offs = range(-minus, plus + 1)
        for h in (0, 1):
            first, second = ("y", "z") if h == 0 else ("z", "y")
            for d in offs:
                if d == 0:
                    continue
                s = 1 if d > 0 else -1
                msgs[(t, h, 1, d, 0)] = ((first, -s), None if abs(d) == 1 else (t, h, 1, d - s, 0))
            for f in offs:
                for d in offs:
                    if d == 0:
                        continue
                    s = 1 if d > 0 else -1
                    if abs(d) == 1:
                        dep = None if f == 0 else (t, h, 1, f, 0)
                    else:
                        dep = (t, h, 2, f, d - s)
                    msgs[(t, h, 2, f, d)] = ((second, -s), dep)
    return msgs


def offset_yz(k):
    _, h, _, f, s = k
    return (f, s) if h == 0 else (s, f)


def priority(k):
    t, h, ph, f, s = k
    if ph == 1:
        return (0 if t == 0 else 0.5, abs(f), 0)
    if t == 0:
        return (1, col_rank(f) + abs(s) if h == 0 else col_rank(s) + abs(f) * 0.1, 0)
    return (2, col_rank(f if h == 0 else s), -abs(s))


def simulate(msgs):
    children, heaps = {}, {}
    for k, (link, dep) in msgs.items():
        heaps.setdefault(link, [])
        if dep is None:
            heapq.heappush(heaps[link], (priority(k), k))
        else:
            children.setdefault(dep, []).append(k)
    queued = {l: 0 for l in heaps}
    until = {l: 0.0 for l in heaps}
    issued, arrival, events, count = [], {}, [], 0

    def fill(link, now):
        nonlocal count
        while queued[link] < DEPTH and heaps[link]:
            _, k = heapq.heappop(heaps[link])
            end = max(now, until[link]) + WIRE
            until[link] = end
            queued[link] += 1
            issued.append((now, k))
            count += 1
            heapq.heappush(events, (end, count, 0, link))
            count += 1
            heapq.heappush(events, (end + HOP, count, 1, k))

    for l in heaps:
        fill(l, 0.0)
    while events:
        now, _, kind, x = heapq.heappop(events)
        if kind == 0:
            queued[x] -= 1
            fill(x, now)
        else:
            arrival[x] = now
            for c in children.get(x, ()):
                link = msgs[c][0]
                heapq.heappush(heaps[link], (priority(c), c))
                fill(link, now)
    return issued, arrival


def plan():
    msgs = build_messages()
    issued, arrival = simulate(msgs)
    steps, waited = [], set()

    def wait_for(keys):
        for k in sorted(keys, key=lambda m: (arrival[m], m)):
            if k not in waited:
                waited.add(k)
                steps.append(("wait", k))

    up_keys = [k for k in msgs if k[0] == 0]
    col_keys = []
    for d in COLS:
        here = [k for k in msgs if k[0] == 1 and offset_yz(k)[0] in ((d, -d) if d == 4 else (d,))]
        col_keys.append(here)
    now, at = 0.0, 0
    tasks = [("norm", i) for i in range(6)]
    ready = {t: 1.5 for t in tasks}
    cost = {"norm": 0.35, "up": 0.5, "D": 0.9, "E": 0.25, "F": 0.15, "G": 0.1}
    up_ready = max(arrival[k] for k in up_keys)
    for i in range(8):
        tasks.append(("up", i))
        ready[("up", i)] = up_ready
    for i in range(8):
        tasks.append(("D", i))
        ready[("D", i)] = max(arrival[k] for k in col_keys[i])
    after = {"D": ("E", 2.0), "E": ("F", 3.0), "F": ("G", 3.5)}
    rank = {"G": 0, "F": 1, "E": 2, "norm": 3, "up": 4, "D": 5}
    while at < len(issued) or tasks:
        if at < len(issued) and issued[at][0] <= now + 0.05:
            k = issued[at][1]
            dep = msgs[k][1]
            if dep is not None:
                wait_for([dep])
            steps.append(("send", k))
            at += 1
            now += 0.01
            continue
        usable = [t for t in tasks if ready[t] <= now]
        firsts = {}
        for t in tasks:
            firsts.setdefault(t[0], t)
        usable = [t for t in usable if firsts[t[0]] == t]
        if any(t[0] == "norm" for t in tasks):
            usable = [t for t in usable if t[0] == "norm"]
        elif any(t[0] == "up" for t in tasks):
            usable = [t for t in usable if t[0] == "up"]
        if usable:
            t = min(usable, key=lambda u: rank[u[0]])
            tasks.remove(t)
            if t[0] == "up":
                wait_for(up_keys)
            if t[0] == "D":
                wait_for(col_keys[t[1]])
            steps.append(t)
            now += cost[t[0]]
            if t[0] in after:
                nxt, lag = after[t[0]]
                tasks.append((nxt, t[1]))
                ready[(nxt, t[1])] = now + lag
            continue
        times = [ready[t] for t in tasks if ready[t] > now]
        if at < len(issued):
            times.append(issued[at][0])
        now = max(now + 0.01, min(times)) if times else now + 0.01
    wait_for(msgs)
    return msgs, steps


def kernel(
    msgs, steps, index,
    tok_hbm, gain_ref, upw_ref, upsc_ref, dnw_ref, dnsc_ref, out_ref,
    tok, up_buf, dn_buf, hid, psend, precv, pown, sbuf, r1, fbuf, gbuf, out_t,
    tok_sem, w_send, w_recv, d_send, d_recv, s_send, s_recv, f_send, f_recv,
):
    fs, tp = lax.axis_index("fs"), lax.axis_index("tp")
    z, y = lax.div(fs, R), lax.rem(fs, R)
    x, c = lax.div(tp, 2), lax.rem(tp, 2)

    def near(axis, g):
        if axis == "y":
            return (z * R + lax.rem(y + (g + R), R), tp)
        if axis == "z":
            return (lax.rem(z + (g + R), R) * R + y, tp)
        return (fs, lax.rem(x + (g + 4), 4) * 2 + c)

    links = {(a, g): near(a, g) for a in "yz" for g in (1, -1)}
    right, left = near("x", 1), near("x", -1)
    partner = (fs, x * 2 + 1 - c)

    barrier = pltpu.get_barrier_semaphore()
    peers = list(links.values()) + [right, left, partner]
    for peer in peers:
        pl.semaphore_signal(barrier, inc=1, device_id=peer, device_id_type=MESH)

    tok_copy = pltpu.make_async_copy(tok_hbm, tok, tok_sem)
    tok_copy.start()

    bufs = (up_buf, dn_buf)
    ys = {d: lax.rem(y + (d + R), R) for d in range(-4, 5)}
    zs = {d: lax.rem(z + (d + R), R) for d in range(-4, 5)}

    def shard_row(dy, dz):
        return zs[dz] * 256 + ys[dy] * 32

    mine = pl.multiple_of(shard_row(0, 0), 32)
    up_buf[pl.ds(mine, 32), :] = upw_ref[...].astype(jnp.bfloat16)
    dn_buf[pl.ds(mine, 32), :] = dnw_ref[...].astype(jnp.bfloat16)

    pl.semaphore_wait(barrier, len(peers))

    def copy_of(k, sending):
        axis, g = msgs[k][0]
        dy, dz = offset_yz(k)
        if sending:
            dy, dz = (dy + g, dz) if axis == "y" else (dy, dz + g)
        row = pl.multiple_of(shard_row(dy, dz) + k[1] * ROWS, ROWS)
        ref = bufs[k[0]].at[pl.ds(row, ROWS), :]
        return pltpu.make_async_remote_copy(
            src_ref=ref, dst_ref=ref,
            send_sem=w_send.at[k[0] * 2 + k[1]], recv_sem=w_recv.at[index[k]],
            device_id=links[(axis, g)], device_id_type=MESH,
        )

    def norm(i):
        if i == 0:
            tok_copy.wait()
        rows = pl.ds(i * 128, 128)
        v = tok[rows, :].astype(jnp.float32)
        scale = lax.rsqrt(jnp.mean(v * v, axis=-1, keepdims=True) + 1e-6)
        tok[rows, :] = (v * scale * gain_ref[...]).astype(jnp.bfloat16)

    def up(i):
        n, half = i // 2, i % 2
        cols = pl.ds(n * 256, 256)
        rows = pl.ds(half * 384, 384)
        pre = jnp.dot(tok[rows, :], up_buf[:, cols], preferred_element_type=jnp.float32)
        pre = jnp.maximum(pre * upsc_ref[:, cols], 0.0)
        hid[cols, rows] = (pre * pre).T.astype(jnp.bfloat16)

    def partial(i, parity):
        row = ys[COLS[i]] * 32 + parity * 256
        lhs = jnp.concatenate(
            [dn_buf[pl.ds(pl.multiple_of(row + k * 512, 32), 32), :] for k in range(4)], axis=0
        )
        return jnp.dot(lhs, hid[...], preferred_element_type=jnp.float32)

    def pair_copy(i):
        return pltpu.make_async_remote_copy(
            src_ref=psend.at[i], dst_ref=precv.at[i], send_sem=d_send, recv_sem=d_recv.at[i],
            device_id=partner, device_id_type=MESH,
        )

    def relay_copy(i, side):
        return pltpu.make_async_remote_copy(
            src_ref=sbuf.at[i, side], dst_ref=r1.at[i, side], send_sem=s_send, recv_sem=s_recv.at[i, side],
            device_id=(right, left)[side], device_id_type=MESH,
        )

    def final_copy(i, side):
        return pltpu.make_async_remote_copy(
            src_ref=fbuf.at[i, side], dst_ref=gbuf.at[i, side], send_sem=f_send, recv_sem=f_recv.at[i, side],
            device_id=(right, left)[side], device_id_type=MESH,
        )

    def step_d(i):
        psend[i] = partial(i, 1 - c).reshape(4, 32, 768).astype(jnp.bfloat16)
        pown[i] = partial(i, c).reshape(4, 32, 768)
        pair_copy(i).start()

    def step_e(i):
        pair_copy(i).wait_recv()
        far = lax.rem(x + 2, 4)
        for q in range(1, 5):
            k = lax.rem(far + q, 4)
            if q == 1:
                total = pown[i, far] + precv[i, far].astype(jnp.float32)
                sbuf[i, 0] = total[:16].astype(jnp.bfloat16)
                sbuf[i, 1] = total[16:].astype(jnp.bfloat16)
            if q < 4:
                pown[i, k] = pown[i, k] + precv[i, k].astype(jnp.float32)
        relay_copy(i, 0).start()
        relay_copy(i, 1).start()

    def step_f(i):
        for side in (0, 1):
            relay_copy(i, side).wait_recv()
            k = lax.rem(x + (1, 3)[side], 4)
            own = pown[i, k]
            extra = r1[i, side].astype(jnp.float32)
            top, bottom = own[:16], own[16:]
            if side == 0:
                top = top + extra
            else:
                bottom = bottom + extra
            fbuf[i, side, :16, :] = top.astype(jnp.bfloat16)
            fbuf[i, side, 16:, :] = bottom.astype(jnp.bfloat16)
            final_copy(i, side).start()

    def step_g(i):
        final_copy(i, 0).wait_recv()
        final_copy(i, 1).wait_recv()
        total = pown[i, x] + gbuf[i, 0].astype(jnp.float32) + gbuf[i, 1].astype(jnp.float32)
        out_t[pl.ds(pl.multiple_of(ys[COLS[i]] * 32, 32), 32), :] = total

    run = {"norm": norm, "up": up, "D": step_d, "E": step_e, "F": step_f, "G": step_g}
    for name, arg in steps:
        if name == "wait":
            copy_of(arg, False).wait_recv()
        elif name == "send":
            copy_of(arg, True).start()
        else:
            run[name](arg)

    scale = dnsc_ref[:, pl.ds(pl.multiple_of(tp * 256, 256), 256)]
    out_ref[...] = (out_t[...].T * scale).astype(jnp.bfloat16)

    def sent(ref, sem):
        pltpu.make_async_copy(ref, ref, sem).wait()

    for t in (0, 1):
        for h in (0, 1):
            sent(bufs[t].at[pl.ds(0, 63 * ROWS), :], w_send.at[t * 2 + h])
    sent(psend, d_send)
    sent(sbuf, s_send)
    sent(fbuf, f_send)


def on_device(tokens, norm_gain, up_weight, up_scale, down_weight, down_scale):
    msgs, steps = plan()
    index = {k: i for i, k in enumerate(msgs)}
    vmem = pl.BlockSpec(memory_space=pltpu.VMEM)
    bf16, f32 = jnp.bfloat16, jnp.float32
    dma = pltpu.SemaphoreType.DMA
    return pl.pallas_call(
        functools.partial(kernel, msgs, steps, index),
        out_shape=jax.ShapeDtypeStruct((768, 256), bf16),
        in_specs=[pl.BlockSpec(memory_space=pl.ANY)] + [vmem] * 5,
        out_specs=vmem,
        scratch_shapes=[
            pltpu.VMEM((768, 2048), bf16),
            pltpu.VMEM((2048, 1024), bf16),
            pltpu.VMEM((2048, 1024), bf16),
            pltpu.VMEM((1024, 768), bf16),
            pltpu.VMEM((8, 4, 32, 768), bf16),
            pltpu.VMEM((8, 4, 32, 768), bf16),
            pltpu.VMEM((8, 4, 32, 768), f32),
            pltpu.VMEM((8, 2, 16, 768), bf16),
            pltpu.VMEM((8, 2, 16, 768), bf16),
            pltpu.VMEM((8, 2, 32, 768), bf16),
            pltpu.VMEM((8, 2, 32, 768), bf16),
            pltpu.VMEM((256, 768), f32),
            dma, dma((4,)), dma((len(msgs),)), dma, dma((8,)), dma, dma((8, 2)), dma, dma((8, 2)),
        ],
        compiler_params=pltpu.CompilerParams(collective_id=0, has_side_effects=True),
    )(
        tokens, norm_gain.reshape(1, -1), up_weight, up_scale.reshape(1, -1), down_weight.T,
        down_scale,
    )


def solution(mesh):
    in_specs = (P("fs", None), P(), P("fs", "tp"), P("tp"), P("tp", "fs"), P())
    return jax.shard_map(
        on_device, mesh=mesh, in_specs=in_specs, out_specs=P("fs", "tp"), check_vma=False
    )
```

time: 245 us -> 84.6 us (0.35)
  waiting for transfers between devices: 213 us -> 0 us
  Pallas kernels: 0 us -> 81.3 us
  between operations: 13.1 us -> 0.01 us
  matrix products: 12.2 us -> 0 us
  other arithmetic: 5.65 us -> 0 us
    all_gather x2 -> x0, waiting for transfers between devices: 172 us -> none  [the longest x1 86.2 us: on_device(): down_full = lax.all_gather(down_cast, 'fs', axis=1, tiled=True)]
    pallas_call x0 -> x1, Pallas kernels: none -> 81.3 us  [on_device(): pl.pallas_call(functools.partial(kernel, msgs, steps, index), out_shape=j...]
    reduce_scatter x1 -> x0, waiting for transfers between devices: 40 us -> none  [on_device(): lax.psum_scatter(rounded, 'tp', scatter_dimension=1, tiled=True)]
    dot_general x1 -> x0, matrix products: 12.2 us -> none  [on_device(): jnp.dot(hidden, down_full, preferred_element_type=jnp.float32) * down_scale]
    convert_element_type x2 -> x0, other arithmetic: 3.07 us -> none  [the longest x1 1.54 us: on_device(): down_cast = down_weight.astype(jnp.bfloat16)]
    reduce_sum x1 -> x0, other arithmetic: 2.57 us -> none  [on_device(): jnp.mean(values * values, axis=-1, keepdims=True) + 1e-06]
  transfers between devices with their start and end apart: 3 -> 0, of which waited for: 3 -> 0; matrix products, arithmetic and copies ran while one was open for 2% -> 0% of each run, Pallas kernels for 0% -> 0%
where the time goes in v1:
time: 84.6 us; the launch traced here: 83.1 us
  Pallas kernels  81.3 us (96%)
  local copies, waits for them, and re-layouts  1.77 us (2%)
    pallas_call x1, Pallas kernels, on_device(): pl.pallas_call(functools.partial(kernel, msgs, steps, index), out_shape=j...  81.3 us
    unnamed x1, local copies, waits for them, and re-layouts  1.77 us

profile of v1, /device:TPU:1, one launch (start us, length us, event | category | flops | bytes accessed | tf_op | source)
XLA Modules:
  0.0 83.1 jit_solution(4807504856324656749)
XLA Ops:
  0.0 81.3 %shard_map.64 = bf16[768,256]{1,0:T(8,128)(2,1)} custom-call(bf16[768,2048]{1,0:T(8,128)(2,1)} %tok_hbm.1, f32[1,2048]{1,0:T(1,128)} %bitcast.4, f32[32,1024]{1,0:T(8,128)} %upw_ref.1, f32[1,1024]{1,0:T(1,128)} %bitcast.5, f32[32,1024]{1,0:T(8,128)} %bitcast.3, f32[1,2048]{1,0:T(1,128)} %dnsc_ref.1), custom_call_target="tpu_custom_call" | custom-call | tf_op jit(solution)/shard_map/pallas_call | solution.py:341
  81.3 1.8 %copy.8 = bf16[768,256]{1,0:T(8,128)(2,1)} copy(bf16[768,256]{1,0:T(8,128)(2,1)} %shard_map.64) | data formatting | bytes 786432

commit v2 on v1

v2 whole, which is shorter than its diff:
```python
import functools
import heapq

import jax
import jax.numpy as jnp
from jax import lax
from jax.experimental import pallas as pl
from jax.experimental.pallas import tpu as pltpu
from jax.sharding import PartitionSpec as P

MESH = pl.DeviceIdType.MESH
R = 8
COLS = (0, 1, -1, 2, -2, 3, -3, 4)
ROWS = 16
DIRECT = (6, 7)
RELAYED = (0, 1, 2, 3, 4, 5)
WIRE, HOP, PAIR, DEPTH = 0.703, 2.6, 1.6, 2
COST = {"norm": 0.22, "U": 0.17, "V": 0.45, "D": 0.57, "E": 0.05, "F": 0.03, "G": 0.02}
BASE, FIRST, NEXT = (1, 16), (0, 1), 1
BLOCK, STEP, LATE, SECOND = (0.2, 1), (1, 1.5), (2, -1), (1, 0.8)


def limits(t):
    return (4, 3) if t == 0 else (3, 4)


def axes(t, h):
    return ("z", "y") if t == h else ("y", "z")


def block_of(k):
    _, h, _, f, s = k
    d = f if h == 0 else s
    return COLS.index(4 if d == -4 else d)


def offset_yz(k):
    t, h, _, f, s = k
    return (f, s) if axes(t, h)[0] == "y" else (s, f)


def build_messages():
    msgs = {}
    for t in (0, 1):
        plus, minus = limits(t)
        offs = range(-minus, plus + 1)
        for h in (0, 1):
            first, second = axes(t, h)
            for d in offs:
                if d == 0:
                    continue
                s = 1 if d > 0 else -1
                msgs[(t, h, 1, d, 0)] = ((first, -s), None if abs(d) == 1 else (t, h, 1, d - s, 0))
            for f in offs:
                for d in offs:
                    if d == 0:
                        continue
                    s = 1 if d > 0 else -1
                    if abs(d) == 1:
                        dep = None if f == 0 else (t, h, 1, f, 0)
                    else:
                        dep = (t, h, 2, f, d - s)
                    msgs[(t, h, 2, f, d)] = ((second, -s), dep)
    return msgs


def priority(k):
    t, h, ph, f, s = k
    if ph == 1:
        return FIRST[t] + NEXT * abs(f)
    if h == 0:
        return BASE[t] + BLOCK[t] * block_of(k) + STEP[t] * abs(s)
    return BASE[t] + SECOND[t] * block_of(k) + 0.01 * abs(f) + LATE[t]


def plan():
    msgs = build_messages()
    children, heaps = {}, {}
    for k, (link, dep) in msgs.items():
        heaps.setdefault(link, [])
        if dep is None:
            heapq.heappush(heaps[link], (priority(k), k))
        else:
            children.setdefault(dep, []).append(k)
    ends = {link: [] for link in heaps}
    wires = [0.0, 0.0]
    arrival, pending, steps, waited, done, ready = {}, [], [], set(), {}, {}
    tasks = [("norm", i) for i in range(6)] + [("U", i) for i in range(32)] + [("D", i) for i in range(8)]
    rank = {"G": 0, "F": 0, "E": 0, "norm": 2, "U": 3, "D": 4}
    blocks = {(t, i): [k for k in msgs if k[0] == t and block_of(k) == i] for t in (0, 1) for i in range(8)}
    now, ups = 0.0, 0

    def wait_for(keys):
        for k in sorted(keys, key=lambda m: (arrival[m], m)):
            if k not in waited:
                waited.add(k)
                steps.append(("wait", k))

    def ready_at(task):
        kind, i = task
        if task not in ready:
            if kind == "norm":
                ready[task] = 0.3
            else:
                need = blocks[(0, i // 4) if kind == "U" else (1, i)]
                before = ("norm", 5) if kind == "U" else ("U", 31)
                if (before in done if kind == "U" else ups == 32) and all(k in arrival for k in need):
                    ready[task] = max(arrival[k] for k in need)
        return ready.get(task, 1e9)

    def on_wires(us):
        for q in (0, 1):
            wires[q] = max(wires[q], now) + us
        return max(wires)

    while True:
        while pending and pending[0][0] <= now:
            for c in children.get(heapq.heappop(pending)[1], ()):
                heapq.heappush(heaps[msgs[c][0]], (priority(c), c))
        best = None
        for link, heap in heaps.items():
            ends[link] = [e for e in ends[link] if e > now]
            if heap and len(ends[link]) < DEPTH:
                key = (len(ends[link]), heap[0][0])
                if best is None or key < best[0]:
                    best = (key, link)
        if best is not None:
            link = best[1]
            k = heapq.heappop(heaps[link])[1]
            if msgs[k][1] is not None:
                wait_for([msgs[k][1]])
            steps.append(("send", k))
            ends[link].append(max([now] + ends[link]) + WIRE)
            arrival[k] = ends[link][-1] + HOP
            heapq.heappush(pending, (arrival[k], k))
            now += 0.012
            continue
        usable = [
            (rank[t[0]], ready_at(t) if t[0] in "UD" else t[1], t) for t in tasks if ready_at(t) <= now
        ]
        if usable:
            task = min(usable)[2]
            tasks.remove(task)
            kind, i = task
            if kind == "U":
                wait_for(blocks[0, i // 4])
                ups += 1
            if kind == "D":
                wait_for(blocks[1, i])
            steps.append(task)
            now += COST["V" if kind == "U" and ups > 28 else kind]
            done[task] = now
            if kind == "D":
                tasks.append(("E", i))
                ready["E", i] = now + PAIR
            if kind == "E" and i in DIRECT:
                tasks.append(("G", i))
                ready["G", i] = on_wires(1.6) + HOP + 0.8
            elif kind == "E":
                tasks.append(("F", i))
                ready["F", i] = on_wires(0.52) + HOP
            if kind == "F":
                tasks.append(("G", i))
                ready["G", i] = on_wires(1.05) + HOP
            continue
        later = [p[0] for p in pending[:1]]
        later += [ends[link][0] for link in heaps if heaps[link] and ends[link]]
        later += [ready_at(t) for t in tasks if now < ready_at(t) < 1e9]
        if not later:
            break
        now = max(now + 1e-6, min(later))
    wait_for(msgs)
    return msgs, steps


def kernel(
    msgs, steps, index,
    tok_hbm, gain_ref, upw_ref, upsc_ref, dnw_ref, dnsc_ref, out_ref,
    tok, up_buf, dn_buf, acc, hid, psend, precv, pown, sbuf, r1, fbuf, gbuf, ebuf, hbuf, out_t,
    tok_sem, w_send, w_recv, d_send, d_recv, s_send, s_recv, f_send, f_recv, e_send, e_recv,
):
    fs, tp = lax.axis_index("fs"), lax.axis_index("tp")
    z, y = lax.div(fs, R), lax.rem(fs, R)
    x, c = lax.div(tp, 2), lax.rem(tp, 2)

    def near(axis, g):
        if axis == "y":
            return (z * R + lax.rem(y + (g + R), R), tp)
        if axis == "z":
            return (lax.rem(z + (g + R), R) * R + y, tp)
        return (fs, lax.rem(x + (g + 4), 4) * 2 + c)

    links = {(a, g): near(a, g) for a in "yz" for g in (1, -1)}
    right, left, far = near("x", 1), near("x", -1), near("x", 2)
    partner = (fs, x * 2 + 1 - c)

    barrier = pltpu.get_barrier_semaphore()
    peers = list(links.values()) + [right, left, far, partner]
    for peer in peers:
        pl.semaphore_signal(barrier, inc=1, device_id=peer, device_id_type=MESH)

    tok_copy = pltpu.make_async_copy(tok_hbm, tok, tok_sem)
    tok_copy.start()

    bufs = (up_buf, dn_buf)
    ys = {d: lax.rem(y + (d + R), R) for d in range(-4, 5)}
    zs = {d: lax.rem(z + (d + R), R) for d in range(-4, 5)}

    def shard_row(dy, dz):
        return zs[dz] * 256 + ys[dy] * 32

    mine = pl.multiple_of(shard_row(0, 0), 32)
    up_buf[pl.ds(mine, 32), :] = upw_ref[...].astype(jnp.bfloat16)
    dn_buf[pl.ds(mine, 32), :] = dnw_ref[...].astype(jnp.bfloat16)

    pl.semaphore_wait(barrier, len(peers))

    def copy_of(k, sending):
        axis, g = msgs[k][0]
        dy, dz = offset_yz(k)
        if sending:
            dy, dz = (dy + g, dz) if axis == "y" else (dy, dz + g)
        row = pl.multiple_of(shard_row(dy, dz) + k[1] * ROWS, ROWS)
        ref = bufs[k[0]].at[pl.ds(row, ROWS), :]
        return pltpu.make_async_remote_copy(
            src_ref=ref, dst_ref=ref,
            send_sem=w_send.at[k[0] * 2 + k[1]], recv_sem=w_recv.at[index[k]],
            device_id=links[(axis, g)], device_id_type=MESH,
        )

    def norm(i):
        if i == 0:
            tok_copy.wait()
        rows = pl.ds(i * 128, 128)
        v = tok[rows, :].astype(jnp.float32)
        scale = lax.rsqrt(jnp.mean(v * v, axis=-1, keepdims=True) + 1e-6)
        tok[rows, :] = (v * scale * gain_ref[...]).astype(jnp.bfloat16)

    seen = [0] * 4

    def up(j):
        i, n = j // 4, j % 4
        cols = pl.ds(n * 256, 256)
        depth = pl.ds(pl.multiple_of(zs[COLS[i]] * 256, 256), 256)
        pre = jnp.dot(tok[:, depth], up_buf[depth, cols], preferred_element_type=jnp.float32)
        if seen[n] > 0:
            pre = acc[:, cols] + pre
        if seen[n] < 7:
            acc[:, cols] = pre
        else:
            pre = jnp.maximum(pre * upsc_ref[:, cols], 0.0)
            hid[cols, :] = (pre * pre).T.astype(jnp.bfloat16)
        seen[n] += 1

    def partial(i, parity):
        row = ys[COLS[i]] * 32 + parity * 256
        lhs = jnp.concatenate(
            [dn_buf[pl.ds(pl.multiple_of(row + k * 512, 32), 32), :] for k in range(4)], axis=0
        )
        return jnp.dot(lhs, hid[...], preferred_element_type=jnp.float32)

    def pair_copy(i):
        return pltpu.make_async_remote_copy(
            src_ref=psend.at[i], dst_ref=precv.at[i], send_sem=d_send, recv_sem=d_recv.at[i],
            device_id=partner, device_id_type=MESH,
        )

    def relay_copy(i, side):
        return pltpu.make_async_remote_copy(
            src_ref=sbuf.at[RELAYED.index(i), side], dst_ref=r1.at[RELAYED.index(i), side],
            send_sem=s_send, recv_sem=s_recv.at[RELAYED.index(i), side],
            device_id=(right, left)[side], device_id_type=MESH,
        )

    def final_copy(i, side):
        return pltpu.make_async_remote_copy(
            src_ref=fbuf.at[RELAYED.index(i), side], dst_ref=gbuf.at[RELAYED.index(i), side],
            send_sem=f_send, recv_sem=f_recv.at[RELAYED.index(i), side],
            device_id=(right, left)[side], device_id_type=MESH,
        )

    def step_d(i):
        psend[i] = partial(i, 1 - c).reshape(4, 32, 768).astype(jnp.bfloat16)
        pown[i] = partial(i, c).reshape(4, 32, 768)
        pair_copy(i).start()

    def direct_copy(i, way):
        return pltpu.make_async_remote_copy(
            src_ref=ebuf.at[DIRECT.index(i), way], dst_ref=hbuf.at[DIRECT.index(i), way],
            send_sem=e_send, recv_sem=e_recv.at[DIRECT.index(i), way],
            device_id=(far, right, left)[way], device_id_type=MESH,
        )

    def summed(i, k):
        return pown[i, k] + precv[i, k].astype(jnp.float32)

    def step_e(i):
        pair_copy(i).wait_recv()
        k_far, k_right, k_left = lax.rem(x + 2, 4), lax.rem(x + 1, 4), lax.rem(x + 3, 4)
        if i in DIRECT:
            for way, k in enumerate((k_far, k_right, k_left)):
                ebuf[DIRECT.index(i), way] = summed(i, k).astype(jnp.bfloat16)
            for way in (0, 1, 2):
                direct_copy(i, way).start()
            pown[i, x] = summed(i, x)
        else:
            r = RELAYED.index(i)
            total = summed(i, k_far).astype(jnp.bfloat16)
            sbuf[r, 0] = total[:16]
            sbuf[r, 1] = total[16:]
            for k in (k_right, k_left):
                pown[i, k] = summed(i, k)
            relay_copy(i, 0).start()
            relay_copy(i, 1).start()
            pown[i, x] = summed(i, x)

    def step_f(i):
        for side in (0, 1):
            relay_copy(i, side).wait_recv()
            k = lax.rem(x + (1, 3)[side], 4)
            own = pown[i, k]
            extra = r1[RELAYED.index(i), side].astype(jnp.float32)
            top, bottom = own[:16], own[16:]
            if side == 0:
                top = top + extra
            else:
                bottom = bottom + extra
            fbuf[RELAYED.index(i), side, :16, :] = top.astype(jnp.bfloat16)
            fbuf[RELAYED.index(i), side, 16:, :] = bottom.astype(jnp.bfloat16)
            final_copy(i, side).start()

    def step_g(i):
        total = pown[i, x]
        if i in DIRECT:
            for way in (0, 1, 2):
                direct_copy(i, way).wait_recv()
                total = total + hbuf[DIRECT.index(i), way].astype(jnp.float32)
        else:
            for side in (0, 1):
                final_copy(i, side).wait_recv()
                total = total + gbuf[RELAYED.index(i), side].astype(jnp.float32)
        out_t[pl.ds(pl.multiple_of(ys[COLS[i]] * 32, 32), 32), :] = total

    run = {"norm": norm, "U": up, "D": step_d, "E": step_e, "F": step_f, "G": step_g}
    for name, arg in steps:
        if name == "wait":
            copy_of(arg, False).wait_recv()
        elif name == "send":
            copy_of(arg, True).start()
        else:
            run[name](arg)

    scale = dnsc_ref[:, pl.ds(pl.multiple_of(tp * 256, 256), 256)]
    out_ref[...] = (out_t[...].T * scale).astype(jnp.bfloat16)

    def sent(ref, sem):
        pltpu.make_async_copy(ref, ref, sem).wait()

    for t in (0, 1):
        for h in (0, 1):
            sent(bufs[t].at[pl.ds(0, 63 * ROWS), :], w_send.at[t * 2 + h])
    sent(psend, d_send)
    sent(sbuf, s_send)
    sent(fbuf, f_send)
    sent(ebuf, e_send)


def on_device(tokens, norm_gain, up_weight, up_scale, down_weight, down_scale):
    msgs, steps = plan()
    index = {k: i for i, k in enumerate(msgs)}
    vmem = pl.BlockSpec(memory_space=pltpu.VMEM)
    bf16, f32 = jnp.bfloat16, jnp.float32
    dma = pltpu.SemaphoreType.DMA
    relayed, direct = len(RELAYED), len(DIRECT)
    return pl.pallas_call(
        functools.partial(kernel, msgs, steps, index),
        out_shape=jax.ShapeDtypeStruct((768, 256), bf16),
        in_specs=[pl.BlockSpec(memory_space=pl.ANY)] + [vmem] * 5,
        out_specs=vmem,
        scratch_shapes=[
            pltpu.VMEM((768, 2048), bf16),
            pltpu.VMEM((2048, 1024), bf16),
            pltpu.VMEM((2048, 1024), bf16),
            pltpu.VMEM((768, 1024), f32),
            pltpu.VMEM((1024, 768), bf16),
            pltpu.VMEM((8, 4, 32, 768), bf16),
            pltpu.VMEM((8, 4, 32, 768), bf16),
            pltpu.VMEM((8, 4, 32, 768), f32),
            pltpu.VMEM((relayed, 2, 16, 768), bf16),
            pltpu.VMEM((relayed, 2, 16, 768), bf16),
            pltpu.VMEM((relayed, 2, 32, 768), bf16),
            pltpu.VMEM((relayed, 2, 32, 768), bf16),
            pltpu.VMEM((direct, 3, 32, 768), bf16),
            pltpu.VMEM((direct, 3, 32, 768), bf16),
            pltpu.VMEM((256, 768), f32),
            dma, dma((4,)), dma((len(msgs),)), dma, dma((8,)),
            dma, dma((relayed, 2)), dma, dma((relayed, 2)), dma, dma((direct, 3)),
        ],
        compiler_params=pltpu.CompilerParams(collective_id=0, has_side_effects=True),
    )(
        tokens, norm_gain.reshape(1, -1), up_weight, up_scale.reshape(1, -1), down_weight.T,
        down_scale,
    )


def solution(mesh):
    in_specs = (P("fs", None), P(), P("fs", "tp"), P("tp"), P("tp", "fs"), P())
    return jax.shard_map(
        on_device, mesh=mesh, in_specs=in_specs, out_specs=P("fs", "tp"), check_vma=False
    )
```

time: 84.6 us -> 78.4 us (0.927); the launches traced: 83.1 us -> 78.2 us
  Pallas kernels: 81.3 us -> 76.4 us
    pallas_call x1, Pallas kernels: 81.3 us -> 76.4 us  [on_device(): pl.pallas_call(functools.partial(kernel, msgs, steps, index), out_shape=j...]
where the time goes in v2:
time: 78.4 us; the launch traced here: 78.2 us
  Pallas kernels  76.4 us (97%)
  local copies, waits for them, and re-layouts  1.77 us (2%)
    pallas_call x1, Pallas kernels, on_device(): pl.pallas_call(functools.partial(kernel, msgs, steps, index), out_shape=j...  76.4 us
    unnamed x1, local copies, waits for them, and re-layouts  1.77 us

profile of v2, /device:TPU:1, one launch (start us, length us, event | category | flops | bytes accessed | tf_op | source)
XLA Modules:
  0.0 78.2 jit_solution(4893901878059905434)
XLA Ops:
  0.0 76.4 %shard_map.64 = bf16[768,256]{1,0:T(8,128)(2,1)} custom-call(bf16[768,2048]{1,0:T(8,128)(2,1)} %tok_hbm.1, f32[1,2048]{1,0:T(1,128)} %bitcast.4, f32[32,1024]{1,0:T(8,128)} %upw_ref.1, f32[1,1024]{1,0:T(1,128)} %bitcast.5, f32[32,1024]{1,0:T(8,128)} %bitcast.3, f32[1,2048]{1,0:T(1,128)} %dnsc_ref.1), custom_call_target="tpu_custom_call" | custom-call | tf_op jit(solution)/shard_map/pallas_call | solution.py:375
  76.4 1.8 %copy.8 = bf16[768,256]{1,0:T(8,128)(2,1)} copy(bf16[768,256]{1,0:T(8,128)(2,1)} %shard_map.64) | data formatting | bytes 786432

commit v3 on v2

--- a/solution.py
+++ b/solution.py
@@ -12,12 +12,10 @@
 R = 8
 COLS = (0, 1, -1, 2, -2, 3, -3, 4)
 ROWS = 16
-DIRECT = (6, 7)
-RELAYED = (0, 1, 2, 3, 4, 5)
-WIRE, HOP, PAIR, DEPTH = 0.703, 2.6, 1.6, 2
-COST = {"norm": 0.22, "U": 0.17, "V": 0.45, "D": 0.57, "E": 0.05, "F": 0.03, "G": 0.02}
-BASE, FIRST, NEXT = (1, 16), (0, 1), 1
-BLOCK, STEP, LATE, SECOND = (0.2, 1), (1, 1.5), (2, -1), (1, 0.8)
+WIRE, HOP, PAIR, DEPTH = 0.703, 2.6, 1.8, 2
+COST = {"norm": 0.22, "U": 0.23, "V": 0.43, "D": 0.57, "E": 0.05, "F": 0.03, "G": 0.02}
+BASE, FIRST, NEXT = (1, 20), (0, 9), 0.1
+BLOCK, STEP, LATE, SECOND = (0, 1), (2, 3), (-2, -2), (0.8, 1.3)
 
 
 def limits(t):
@@ -153,10 +151,7 @@
             if kind == "D":
                 tasks.append(("E", i))
                 ready["E", i] = now + PAIR
-            if kind == "E" and i in DIRECT:
-                tasks.append(("G", i))
-                ready["G", i] = on_wires(1.6) + HOP + 0.8
-            elif kind == "E":
+            if kind == "E":
                 tasks.append(("F", i))
                 ready["F", i] = on_wires(0.52) + HOP
             if kind == "F":
@@ -175,9 +170,10 @@
 
 def kernel(
     msgs, steps, index,
-    tok_hbm, gain_ref, upw_ref, upsc_ref, dnw_ref, dnsc_ref, out_ref,
-    tok, up_buf, dn_buf, acc, hid, psend, precv, pown, sbuf, r1, fbuf, gbuf, ebuf, hbuf, out_t,
-    tok_sem, w_send, w_recv, d_send, d_recv, s_send, s_recv, f_send, f_recv, e_send, e_recv,
+    tok_hbm, gain_hbm, upw_hbm, upsc_hbm, dnw_hbm, dnsc_hbm, out_ref,
+    tok, gain_ref, upw_ref, upsc_ref, dnw_ref, dnsc_ref,
+    up_buf, dn_buf, acc, hid, psend, precv, pown, sbuf, r1, fbuf, gbuf, out_t,
+    in_sem, w_send, w_recv, d_send, d_recv, s_send, s_recv, f_send, f_recv,
 ):
     fs, tp = lax.axis_index("fs"), lax.axis_index("tp")
     z, y = lax.div(fs, R), lax.rem(fs, R)
@@ -191,16 +187,21 @@
         return (fs, lax.rem(x + (g + 4), 4) * 2 + c)
 
     links = {(a, g): near(a, g) for a in "yz" for g in (1, -1)}
-    right, left, far = near("x", 1), near("x", -1), near("x", 2)
+    right, left = near("x", 1), near("x", -1)
     partner = (fs, x * 2 + 1 - c)
 
     barrier = pltpu.get_barrier_semaphore()
-    peers = list(links.values()) + [right, left, far, partner]
+    peers = list(links.values()) + [right, left, partner]
     for peer in peers:
         pl.semaphore_signal(barrier, inc=1, device_id=peer, device_id_type=MESH)
 
-    tok_copy = pltpu.make_async_copy(tok_hbm, tok, tok_sem)
-    tok_copy.start()
+    pairs = (
+        (upw_hbm, upw_ref), (dnw_hbm, dnw_ref), (tok_hbm, tok),
+        (gain_hbm, gain_ref), (upsc_hbm, upsc_ref), (dnsc_hbm, dnsc_ref),
+    )
+    loads = [pltpu.make_async_copy(a, b, in_sem.at[n]) for n, (a, b) in enumerate(pairs)]
+    for load in loads:
+        load.start()
 
     bufs = (up_buf, dn_buf)
     ys = {d: lax.rem(y + (d + R), R) for d in range(-4, 5)}
@@ -210,7 +211,9 @@
         return zs[dz] * 256 + ys[dy] * 32
 
     mine = pl.multiple_of(shard_row(0, 0), 32)
+    loads[0].wait()
     up_buf[pl.ds(mine, 32), :] = upw_ref[...].astype(jnp.bfloat16)
+    loads[1].wait()
     dn_buf[pl.ds(mine, 32), :] = dnw_ref[...].astype(jnp.bfloat16)
 
     pl.semaphore_wait(barrier, len(peers))
@@ -230,7 +233,8 @@
 
     def norm(i):
         if i == 0:
-            tok_copy.wait()
+            for load in loads[2:]:
+                load.wait()
         rows = pl.ds(i * 128, 128)
         v = tok[rows, :].astype(jnp.float32)
         scale = lax.rsqrt(jnp.mean(v * v, axis=-1, keepdims=True) + 1e-6)
@@ -267,15 +271,15 @@
 
     def relay_copy(i, side):
         return pltpu.make_async_remote_copy(
-            src_ref=sbuf.at[RELAYED.index(i), side], dst_ref=r1.at[RELAYED.index(i), side],
-            send_sem=s_send, recv_sem=s_recv.at[RELAYED.index(i), side],
+            src_ref=sbuf.at[i, side], dst_ref=r1.at[i, side],
+            send_sem=s_send, recv_sem=s_recv.at[i, side],
             device_id=(right, left)[side], device_id_type=MESH,
         )
 
     def final_copy(i, side):
         return pltpu.make_async_remote_copy(
-            src_ref=fbuf.at[RELAYED.index(i), side], dst_ref=gbuf.at[RELAYED.index(i), side],
-            send_sem=f_send, recv_sem=f_recv.at[RELAYED.index(i), side],
+            src_ref=fbuf.at[i, side], dst_ref=gbuf.at[i, side],
+            send_sem=f_send, recv_sem=f_recv.at[i, side],
             device_id=(right, left)[side], device_id_type=MESH,
         )
 
@@ -284,61 +288,41 @@
         pown[i] = partial(i, c).reshape(4, 32, 768)
         pair_copy(i).start()
 
-    def direct_copy(i, way):
-        return pltpu.make_async_remote_copy(
-            src_ref=ebuf.at[DIRECT.index(i), way], dst_ref=hbuf.at[DIRECT.index(i), way],
-            send_sem=e_send, recv_sem=e_recv.at[DIRECT.index(i), way],
-            device_id=(far, right, left)[way], device_id_type=MESH,
-        )
-
     def summed(i, k):
         return pown[i, k] + precv[i, k].astype(jnp.float32)
 
     def step_e(i):
         pair_copy(i).wait_recv()
         k_far, k_right, k_left = lax.rem(x + 2, 4), lax.rem(x + 1, 4), lax.rem(x + 3, 4)
-        if i in DIRECT:
-            for way, k in enumerate((k_far, k_right, k_left)):
-                ebuf[DIRECT.index(i), way] = summed(i, k).astype(jnp.bfloat16)
-            for way in (0, 1, 2):
-                direct_copy(i, way).start()
-            pown[i, x] = summed(i, x)
-        else:
-            r = RELAYED.index(i)
-            total = summed(i, k_far).astype(jnp.bfloat16)
-            sbuf[r, 0] = total[:16]
-            sbuf[r, 1] = total[16:]
-            for k in (k_right, k_left):
-                pown[i, k] = summed(i, k)
-            relay_copy(i, 0).start()
-            relay_copy(i, 1).start()
-            pown[i, x] = summed(i, x)
+        total = summed(i, k_far).astype(jnp.bfloat16)
+        sbuf[i, 0] = total[:16]
+        sbuf[i, 1] = total[16:]
+        for k in (k_right, k_left):
+            pown[i, k] = summed(i, k)
+        relay_copy(i, 0).start()
+        relay_copy(i, 1).start()
+        pown[i, x] = summed(i, x)
 
     def step_f(i):
         for side in (0, 1):
             relay_copy(i, side).wait_recv()
             k = lax.rem(x + (1, 3)[side], 4)
             own = pown[i, k]
-            extra = r1[RELAYED.index(i), side].astype(jnp.float32)
+            extra = r1[i, side].astype(jnp.float32)
             top, bottom = own[:16], own[16:]
             if side == 0:
                 top = top + extra
             else:
                 bottom = bottom + extra
-            fbuf[RELAYED.index(i), side, :16, :] = top.astype(jnp.bfloat16)
-            fbuf[RELAYED.index(i), side, 16:, :] = bottom.astype(jnp.bfloat16)
+            fbuf[i, side, :16, :] = top.astype(jnp.bfloat16)
+            fbuf[i, side, 16:, :] = bottom.astype(jnp.bfloat16)
             final_copy(i, side).start()
 
     def step_g(i):
         total = pown[i, x]
-        if i in DIRECT:
-            for way in (0, 1, 2):
-                direct_copy(i, way).wait_recv()
-                total = total + hbuf[DIRECT.index(i), way].astype(jnp.float32)
-        else:
-            for side in (0, 1):
-                final_copy(i, side).wait_recv()
-                total = total + gbuf[RELAYED.index(i), side].astype(jnp.float32)
+        for side in (0, 1):
+            final_copy(i, side).wait_recv()
+            total = total + gbuf[i, side].astype(jnp.float32)
         out_t[pl.ds(pl.multiple_of(ys[COLS[i]] * 32, 32), 32), :] = total
 
     run = {"norm": norm, "U": up, "D": step_d, "E": step_e, "F": step_f, "G": step_g}
@@ -362,23 +346,33 @@
     sent(psend, d_send)
     sent(sbuf, s_send)
     sent(fbuf, f_send)
-    sent(ebuf, e_send)
+
+
+def scoped_kernel(msgs, steps, index, *refs):
+    dma = pltpu.SemaphoreType.DMA
+    pl.run_scoped(
+        functools.partial(kernel, msgs, steps, index, *refs),
+        dma((6,)), dma((4,)), dma((len(msgs),)), dma, dma((8,)),
+        dma, dma((8, 2)), dma, dma((8, 2)),
+    )
 
 
 def on_device(tokens, norm_gain, up_weight, up_scale, down_weight, down_scale):
     msgs, steps = plan()
     index = {k: i for i, k in enumerate(msgs)}
-    vmem = pl.BlockSpec(memory_space=pltpu.VMEM)
     bf16, f32 = jnp.bfloat16, jnp.float32
-    dma = pltpu.SemaphoreType.DMA
-    relayed, direct = len(RELAYED), len(DIRECT)
     return pl.pallas_call(
-        functools.partial(kernel, msgs, steps, index),
-        out_shape=jax.ShapeDtypeStruct((768, 256), bf16),
-        in_specs=[pl.BlockSpec(memory_space=pl.ANY)] + [vmem] * 5,
-        out_specs=vmem,
+        functools.partial(scoped_kernel, msgs, steps, index),
+        out_shape=pltpu.VMEM((768, 256), bf16),
+        in_specs=[pl.BlockSpec(memory_space=pl.ANY)] * 6,
+        out_specs=pl.BlockSpec(memory_space=pltpu.VMEM),
         scratch_shapes=[
             pltpu.VMEM((768, 2048), bf16),
+            pltpu.VMEM((1, 2048), f32),
+            pltpu.VMEM((32, 1024), f32),
+            pltpu.VMEM((1, 1024), f32),
+            pltpu.VMEM((32, 1024), f32),
+            pltpu.VMEM((1, 2048), f32),
             pltpu.VMEM((2048, 1024), bf16),
             pltpu.VMEM((2048, 1024), bf16),
             pltpu.VMEM((768, 1024), f32),
@@ -386,15 +380,11 @@
             pltpu.VMEM((8, 4, 32, 768), bf16),
             pltpu.VMEM((8, 4, 32, 768), bf16),
             pltpu.VMEM((8, 4, 32, 768), f32),
-            pltpu.VMEM((relayed, 2, 16, 768), bf16),
-            pltpu.VMEM((relayed, 2, 16, 768), bf16),
-            pltpu.VMEM((relayed, 2, 32, 768), bf16),
-            pltpu.VMEM((relayed, 2, 32, 768), bf16),
-            pltpu.VMEM((direct, 3, 32, 768), bf16),
-            pltpu.VMEM((direct, 3, 32, 768), bf16),
+            pltpu.VMEM((8, 2, 16, 768), bf16),
+            pltpu.VMEM((8, 2, 16, 768), bf16),
+            pltpu.VMEM((8, 2, 32, 768), bf16),
+            pltpu.VMEM((8, 2, 32, 768), bf16),
             pltpu.VMEM((256, 768), f32),
-            dma, dma((4,)), dma((len(msgs),)), dma, dma((8,)),
-            dma, dma((relayed, 2)), dma, dma((relayed, 2)), dma, dma((direct, 3)),
         ],
         compiler_params=pltpu.CompilerParams(collective_id=0, has_side_effects=True),
     )(

time: 78.4 us -> 72.7 us (0.927)
  Pallas kernels: 76.4 us -> 71.9 us
  local copies, waits for them, and re-layouts: 1.77 us -> 0.75 us
    pallas_call x1, Pallas kernels: 76.4 us -> 71.9 us  [on_device(): pl.pallas_call(functools.partial(scoped_kernel, msgs, steps, index), out_...]
    unnamed x1, local copies, waits for them, and re-layouts: 1.77 us -> 0.75 us
where the time goes in v3:
time: 72.7 us; the launch traced here: 72.6 us
  Pallas kernels  71.9 us (99%)
  local copies, waits for them, and re-layouts  0.75 us (1%)
    pallas_call x1, Pallas kernels, on_device(): pl.pallas_call(functools.partial(scoped_kernel, msgs, steps, index), out_...  71.9 us

profile of v3, /device:TPU:1, one launch (start us, length us, event | category | flops | bytes accessed | tf_op | source)
XLA Modules:
  0.0 72.6 jit_solution(12130713103639375326)
XLA Ops:
  0.0 71.9 %shard_map.64 = bf16[768,256]{1,0:T(8,128)(2,1)S(1)} custom-call(bf16[768,2048]{1,0:T(8,128)(2,1)} %refs_0_.1, f32[1,2048]{1,0:T(1,128)} %bitcast.4, f32[32,1024]{1,0:T(8,128)} %refs_2_.1, f32[1,1024]{1,0:T(1,128)} %bitcast.5, f32[32,1024]{1,0:T(8,128)} %bitcast.3, f32[1,2048]{1,0:T(1,128)} %refs_5_.1), custom_call_target="tpu_custom_call" | custom-call | tf_op jit(solution)/shard_map/pallas_call | solution.py:364
  71.9 0.7 %copy.8 = bf16[768,256]{1,0:T(8,128)(2,1)} copy(bf16[768,256]{1,0:T(8,128)(2,1)S(1)} %shard_map.64) | data formatting | bytes 786432

commit v4 on v3

--- a/solution.py
+++ b/solution.py
@@ -12,18 +12,28 @@
 R = 8
 COLS = (0, 1, -1, 2, -2, 3, -3, 4)
 ROWS = 16
-WIRE, HOP, PAIR, DEPTH = 0.703, 2.6, 1.8, 2
-COST = {"norm": 0.22, "U": 0.23, "V": 0.43, "D": 0.57, "E": 0.05, "F": 0.03, "G": 0.02}
-BASE, FIRST, NEXT = (1, 20), (0, 9), 0.1
-BLOCK, STEP, LATE, SECOND = (0, 1), (2, 3), (-2, -2), (0.8, 1.3)
-
-
-def limits(t):
-    return (4, 3) if t == 0 else (3, 4)
+WIRE, HOP, WAY, PAIR, DEPTH = 0.703, 2.8, 3.1, 1.8, 2
+STEP = 16.31
+COST = {"norm": 0.22, "U": 0.28, "V": 0.44, "D": 0.45, "E": 0.05, "F": 0.03, "G": 0.02}
+
+DUE = (
+    (
+        (-1.3, -38.8, 6.0, -11.0, -24.6, 19.5, -16.2, -18.6),
+        (-15.4, 23.0, 56.1, 14.3, 17.4, -10.9, 5.5, 7.4),
+    ),
+    (
+        (61.4, 19.4, 63.9, 44.6, 47.9, 26.6, 68.4, 62.4),
+        (23.2, 34.6, 92.2, 95.6, 155.2, 56.9, 54.7, 59.9),
+    ),
+)
 
 
 def axes(t, h):
     return ("z", "y") if t == h else ("y", "z")
+
+
+def offsets(t, f=0):
+    return range(-3, 5) if (t + f) % 2 == 0 else range(-4, 4)
 
 
 def block_of(k):
@@ -40,53 +50,52 @@
 def build_messages():
     msgs = {}
     for t in (0, 1):
-        plus, minus = limits(t)
-        offs = range(-minus, plus + 1)
         for h in (0, 1):
             first, second = axes(t, h)
-            for d in offs:
-                if d == 0:
-                    continue
+            for d in offsets(t):
                 s = 1 if d > 0 else -1
-                msgs[(t, h, 1, d, 0)] = ((first, -s), None if abs(d) == 1 else (t, h, 1, d - s, 0))
-            for f in offs:
-                for d in offs:
-                    if d == 0:
-                        continue
+                if d:
+                    msgs[(t, h, 1, d, 0)] = ((first, -s), None if abs(d) == 1 else (t, h, 1, d - s, 0))
+            for f in offsets(t):
+                for d in offsets(t, f):
                     s = 1 if d > 0 else -1
                     if abs(d) == 1:
                         dep = None if f == 0 else (t, h, 1, f, 0)
                     else:
                         dep = (t, h, 2, f, d - s)
-                    msgs[(t, h, 2, f, d)] = ((second, -s), dep)
+                    if d:
+                        msgs[(t, h, 2, f, d)] = ((second, -s), dep)
     return msgs
 
 
-def priority(k):
-    t, h, ph, f, s = k
-    if ph == 1:
-        return FIRST[t] + NEXT * abs(f)
-    if h == 0:
-        return BASE[t] + BLOCK[t] * block_of(k) + STEP[t] * abs(s)
-    return BASE[t] + SECOND[t] * block_of(k) + 0.01 * abs(f) + LATE[t]
-
-
-def plan():
+def due_times(msgs):
+    due = {}
+    for k in sorted(msgs, key=lambda m: -abs(m[3]) - abs(m[4])):
+        due[k] = min(due.get(k, 1e9), DUE[k[0]][k[1]][block_of(k)])
+        dep = msgs[k][1]
+        if dep is not None:
+            due[dep] = min(due.get(dep, 1e9), due[k] - STEP)
+    return due
+
+
+def plan(log=None):
     msgs = build_messages()
     children, heaps = {}, {}
+    due = due_times(msgs)
     for k, (link, dep) in msgs.items():
         heaps.setdefault(link, [])
         if dep is None:
-            heapq.heappush(heaps[link], (priority(k), k))
+            heapq.heappush(heaps[link], (due[k], k))
         else:
             children.setdefault(dep, []).append(k)
     ends = {link: [] for link in heaps}
     wires = [0.0, 0.0]
-    arrival, pending, steps, waited, done, ready = {}, [], [], set(), {}, {}
-    tasks = [("norm", i) for i in range(6)] + [("U", i) for i in range(32)] + [("D", i) for i in range(8)]
-    rank = {"G": 0, "F": 0, "E": 0, "norm": 2, "U": 3, "D": 4}
-    blocks = {(t, i): [k for k in msgs if k[0] == t and block_of(k) == i] for t in (0, 1) for i in range(8)}
-    now, ups = 0.0, 0
+    arrival, pending, steps, waited, ready = {}, [], [], set(), {}
+    tasks = [("norm", i) for i in range(6)] + [("U", i) for i in range(32)] + [("D", i) for i in range(16)]
+    rank = {"G": 1, "F": 0, "E": 0, "norm": 2, "U": 3, "D": 4}
+    blocks = {(0, i): [k for k in msgs if k[0] == 0 and block_of(k) == i] for i in range(8)}
+    blocks.update({(1, i): [k for k in msgs if k[:2] == (1, i % 2) and block_of(k) == i // 2] for i in range(16)})
+    now, ups, norms = 0.0, 0, 0
 
     def wait_for(keys):
         for k in sorted(keys, key=lambda m: (arrival[m], m)):
@@ -101,8 +110,7 @@
                 ready[task] = 0.3
             else:
                 need = blocks[(0, i // 4) if kind == "U" else (1, i)]
-                before = ("norm", 5) if kind == "U" else ("U", 31)
-                if (before in done if kind == "U" else ups == 32) and all(k in arrival for k in need):
+                if (norms == 6 if kind == "U" else ups == 32) and all(k in arrival for k in need):
                     ready[task] = max(arrival[k] for k in need)
         return ready.get(task, 1e9)
 
@@ -113,8 +121,9 @@
 
     while True:
         while pending and pending[0][0] <= now:
-            for c in children.get(heapq.heappop(pending)[1], ()):
-                heapq.heappush(heaps[msgs[c][0]], (priority(c), c))
+            k = heapq.heappop(pending)[1]
+            for c in children.get(k, ()):
+                heapq.heappush(heaps[msgs[c][0]], (due[c], c))
         best = None
         for link, heap in heaps.items():
             ends[link] = [e for e in ends[link] if e > now]
@@ -140,23 +149,25 @@
             task = min(usable)[2]
             tasks.remove(task)
             kind, i = task
+            norms += kind == "norm"
             if kind == "U":
                 wait_for(blocks[0, i // 4])
                 ups += 1
             if kind == "D":
                 wait_for(blocks[1, i])
             steps.append(task)
+            if log is not None:
+                log.append((now, task))
             now += COST["V" if kind == "U" and ups > 28 else kind]
-            done[task] = now
             if kind == "D":
                 tasks.append(("E", i))
                 ready["E", i] = now + PAIR
             if kind == "E":
                 tasks.append(("F", i))
-                ready["F", i] = on_wires(0.52) + HOP
+                ready["F", i] = on_wires(0.26) + WAY
             if kind == "F":
                 tasks.append(("G", i))
-                ready["G", i] = on_wires(1.05) + HOP
+                ready["G", i] = on_wires(0.52) + WAY + 0.8
             continue
         later = [p[0] for p in pending[:1]]
         later += [ends[link][0] for link in heaps if heaps[link] and ends[link]]
@@ -165,6 +176,8 @@
             break
         now = max(now + 1e-6, min(later))
     wait_for(msgs)
+    if log is not None:
+        log.append((now, max(arrival.values()), max(v for k, v in arrival.items() if k[0] == 0)))
     return msgs, steps
 
 
@@ -256,13 +269,6 @@
             hid[cols, :] = (pre * pre).T.astype(jnp.bfloat16)
         seen[n] += 1
 
-    def partial(i, parity):
-        row = ys[COLS[i]] * 32 + parity * 256
-        lhs = jnp.concatenate(
-            [dn_buf[pl.ds(pl.multiple_of(row + k * 512, 32), 32), :] for k in range(4)], axis=0
-        )
-        return jnp.dot(lhs, hid[...], preferred_element_type=jnp.float32)
-
     def pair_copy(i):
         return pltpu.make_async_remote_copy(
             src_ref=psend.at[i], dst_ref=precv.at[i], send_sem=d_send, recv_sem=d_recv.at[i],
@@ -271,21 +277,25 @@
 
     def relay_copy(i, side):
         return pltpu.make_async_remote_copy(
-            src_ref=sbuf.at[i, side], dst_ref=r1.at[i, side],
-            send_sem=s_send, recv_sem=s_recv.at[i, side],
+            src_ref=sbuf.at[i, side], dst_ref=r1.at[i, side], send_sem=s_send, recv_sem=s_recv.at[i, side],
             device_id=(right, left)[side], device_id_type=MESH,
         )
 
     def final_copy(i, side):
         return pltpu.make_async_remote_copy(
-            src_ref=fbuf.at[i, side], dst_ref=gbuf.at[i, side],
-            send_sem=f_send, recv_sem=f_recv.at[i, side],
+            src_ref=fbuf.at[i, side], dst_ref=gbuf.at[i, side], send_sem=f_send, recv_sem=f_recv.at[i, side],
             device_id=(right, left)[side], device_id_type=MESH,
         )
 
+    def row_in_block(i):
+        return ys[COLS[i // 2]] * 32 + (i % 2) * ROWS
+
     def step_d(i):
-        psend[i] = partial(i, 1 - c).reshape(4, 32, 768).astype(jnp.bfloat16)
-        pown[i] = partial(i, c).reshape(4, 32, 768)
+        rows = [row_in_block(i) + parity * 256 + k * 512 for parity in (1 - c, c) for k in range(4)]
+        lhs = jnp.concatenate([dn_buf[pl.ds(pl.multiple_of(r, ROWS), ROWS), :] for r in rows], axis=0)
+        part = jnp.dot(lhs, hid[...], preferred_element_type=jnp.float32)
+        psend[i] = part[:64].reshape(4, ROWS, 768).astype(jnp.bfloat16)
+        pown[i] = part[64:].reshape(4, ROWS, 768)
         pair_copy(i).start()
 
     def summed(i, k):
@@ -295,8 +305,8 @@
         pair_copy(i).wait_recv()
         k_far, k_right, k_left = lax.rem(x + 2, 4), lax.rem(x + 1, 4), lax.rem(x + 3, 4)
         total = summed(i, k_far).astype(jnp.bfloat16)
-        sbuf[i, 0] = total[:16]
-        sbuf[i, 1] = total[16:]
+        sbuf[i, 0] = total[:, :384]
+        sbuf[i, 1] = total[:, 384:]
         for k in (k_right, k_left):
             pown[i, k] = summed(i, k)
         relay_copy(i, 0).start()
@@ -306,16 +316,15 @@
     def step_f(i):
         for side in (0, 1):
             relay_copy(i, side).wait_recv()
-            k = lax.rem(x + (1, 3)[side], 4)
-            own = pown[i, k]
+            own = pown[i, lax.rem(x + (1, 3)[side], 4)]
             extra = r1[i, side].astype(jnp.float32)
-            top, bottom = own[:16], own[16:]
+            head, tail = own[:, :384], own[:, 384:]
             if side == 0:
-                top = top + extra
+                head = head + extra
             else:
-                bottom = bottom + extra
-            fbuf[i, side, :16, :] = top.astype(jnp.bfloat16)
-            fbuf[i, side, 16:, :] = bottom.astype(jnp.bfloat16)
+                tail = tail + extra
+            fbuf[i, side, :, :384] = head.astype(jnp.bfloat16)
+            fbuf[i, side, :, 384:] = tail.astype(jnp.bfloat16)
             final_copy(i, side).start()
 
     def step_g(i):
@@ -323,7 +332,7 @@
         for side in (0, 1):
             final_copy(i, side).wait_recv()
             total = total + gbuf[i, side].astype(jnp.float32)
-        out_t[pl.ds(pl.multiple_of(ys[COLS[i]] * 32, 32), 32), :] = total
+        out_t[pl.ds(pl.multiple_of(row_in_block(i), ROWS), ROWS), :] = total
 
     run = {"norm": norm, "U": up, "D": step_d, "E": step_e, "F": step_f, "G": step_g}
     for name, arg in steps:
@@ -352,8 +361,8 @@
     dma = pltpu.SemaphoreType.DMA
     pl.run_scoped(
         functools.partial(kernel, msgs, steps, index, *refs),
-        dma((6,)), dma((4,)), dma((len(msgs),)), dma, dma((8,)),
-        dma, dma((8, 2)), dma, dma((8, 2)),
+        dma((6,)), dma((4,)), dma((len(msgs),)), dma, dma((16,)),
+        dma, dma((16, 2)), dma, dma((16, 2)),
     )
 
 
@@ -377,13 +386,13 @@
             pltpu.VMEM((2048, 1024), bf16),
             pltpu.VMEM((768, 1024), f32),
             pltpu.VMEM((1024, 768), bf16),
-            pltpu.VMEM((8, 4, 32, 768), bf16),
-            pltpu.VMEM((8, 4, 32, 768), bf16),
-            pltpu.VMEM((8, 4, 32, 768), f32),
-            pltpu.VMEM((8, 2, 16, 768), bf16),
-            pltpu.VMEM((8, 2, 16, 768), bf16),
-            pltpu.VMEM((8, 2, 32, 768), bf16),
-            pltpu.VMEM((8, 2, 32, 768), bf16),
+            pltpu.VMEM((16, 4, 16, 768), bf16),
+            pltpu.VMEM((16, 4, 16, 768), bf16),
+            pltpu.VMEM((16, 4, 16, 768), f32),
+            pltpu.VMEM((16, 2, 16, 384), bf16),
+            pltpu.VMEM((16, 2, 16, 384), bf16),
+            pltpu.VMEM((16, 2, 16, 768), bf16),
+            pltpu.VMEM((16, 2, 16, 768), bf16),
             pltpu.VMEM((256, 768), f32),
         ],
         compiler_params=pltpu.CompilerParams(collective_id=0, has_side_effects=True),

time: 72.7 us -> 70.9 us (0.975)
  Pallas kernels: 71.9 us -> 70.1 us
    pallas_call x1, Pallas kernels: 71.9 us -> 70.1 us  [on_device(): pl.pallas_call(functools.partial(scoped_kernel, msgs, steps, index), out_...]
where the time goes in v4:
time: 70.9 us; the launch traced here: 70.8 us
  Pallas kernels  70.1 us (99%)
  local copies, waits for them, and re-layouts  0.75 us (1%)
    pallas_call x1, Pallas kernels, on_device(): pl.pallas_call(functools.partial(scoped_kernel, msgs, steps, index), out_...  70.1 us

profile of v4, /device:TPU:1, one launch (start us, length us, event | category | flops | bytes accessed | tf_op | source)
XLA Modules:
  0.0 70.8 jit_solution(15419045857808469804)
XLA Ops:
  0.0 70.1 %shard_map.64 = bf16[768,256]{1,0:T(8,128)(2,1)S(1)} custom-call(bf16[768,2048]{1,0:T(8,128)(2,1)} %refs_0_.1, f32[1,2048]{1,0:T(1,128)} %bitcast.4, f32[32,1024]{1,0:T(8,128)} %refs_2_.1, f32[1,1024]{1,0:T(1,128)} %bitcast.5, f32[32,1024]{1,0:T(8,128)} %bitcast.3, f32[1,2048]{1,0:T(1,128)} %refs_5_.1), custom_call_target="tpu_custom_call" | custom-call | tf_op jit(solution)/shard_map/pallas_call | solution.py:373
  70.1 0.7 %copy.8 = bf16[768,256]{1,0:T(8,128)(2,1)} copy(bf16[768,256]{1,0:T(8,128)(2,1)S(1)} %shard_map.64) | data formatting | bytes 786432

commit v5 on v4

--- a/solution.py
+++ b/solution.py
@@ -13,17 +13,18 @@
 COLS = (0, 1, -1, 2, -2, 3, -3, 4)
 ROWS = 16
 WIRE, HOP, WAY, PAIR, DEPTH = 0.703, 2.8, 3.1, 1.8, 2
-STEP = 16.31
-COST = {"norm": 0.22, "U": 0.28, "V": 0.44, "D": 0.45, "E": 0.05, "F": 0.03, "G": 0.02}
+STEP = 18.94
+COST = {"norm": 0.22, "U": 0.28, "V": 0.44, "D": 0.45, "E": 0.05, "F": 0.03, "G": 0.02, "L": 0.5, "M": 0.06}
+LAST = 4
 
 DUE = (
     (
-        (-1.3, -38.8, 6.0, -11.0, -24.6, 19.5, -16.2, -18.6),
-        (-15.4, 23.0, 56.1, 14.3, 17.4, -10.9, 5.5, 7.4),
+        (4.1, -34.3, 16.5, -24.1, -49.3, -7.6, -41.5, -31.4),
+        (-30.9, 12.5, 39.1, 34.0, 16.3, 4.0, 3.6, -15.7),
     ),
     (
-        (61.4, 19.4, 63.9, 44.6, 47.9, 26.6, 68.4, 62.4),
-        (23.2, 34.6, 92.2, 95.6, 155.2, 56.9, 54.7, 59.9),
+        (64.3, 22.9, 71.7, 33.2, 46.6, 25.8, 72.8, 48.8),
+        (36.3, 48.7, 88.5, 92.2, 145.0, 61.6, 55.4, 66.4),
     ),
 )
 
@@ -92,7 +93,7 @@
     wires = [0.0, 0.0]
     arrival, pending, steps, waited, ready = {}, [], [], set(), {}
     tasks = [("norm", i) for i in range(6)] + [("U", i) for i in range(32)] + [("D", i) for i in range(16)]
-    rank = {"G": 1, "F": 0, "E": 0, "norm": 2, "U": 3, "D": 4}
+    rank = {"G": 1, "M": 0, "F": 0, "E": 0, "norm": 2, "U": 3, "D": 4}
     blocks = {(0, i): [k for k in msgs if k[0] == 0 and block_of(k) == i] for i in range(8)}
     blocks.update({(1, i): [k for k in msgs if k[:2] == (1, i % 2) and block_of(k) == i // 2] for i in range(16)})
     now, ups, norms = 0.0, 0, 0
@@ -155,6 +156,8 @@
                 ups += 1
             if kind == "D":
                 wait_for(blocks[1, i])
+            if kind == "D" and sum(t[0] == "D" for t in tasks) < LAST:
+                kind, task = "L", ("L", i)
             steps.append(task)
             if log is not None:
                 log.append((now, task))
@@ -165,7 +168,10 @@
             if kind == "E":
                 tasks.append(("F", i))
                 ready["F", i] = on_wires(0.26) + WAY
-            if kind == "F":
+            if kind == "L":
+                tasks.append(("M", i))
+                ready["M", i] = max(now + PAIR, on_wires(0.52) + WAY)
+            if kind in "FM":
                 tasks.append(("G", i))
                 ready["G", i] = on_wires(0.52) + WAY + 0.8
             continue
@@ -185,8 +191,8 @@
     msgs, steps, index,
     tok_hbm, gain_hbm, upw_hbm, upsc_hbm, dnw_hbm, dnsc_hbm, out_ref,
     tok, gain_ref, upw_ref, upsc_ref, dnw_ref, dnsc_ref,
-    up_buf, dn_buf, acc, hid, psend, precv, pown, sbuf, r1, fbuf, gbuf, out_t,
-    in_sem, w_send, w_recv, d_send, d_recv, s_send, s_recv, f_send, f_recv,
+    up_buf, dn_buf, acc, hid, psend, precv, pown, sbuf, r1, r2, fbuf, gbuf, out_t,
+    in_sem, w_send, w_recv, d_send, d_recv, s_send, s_recv, f_send, f_recv, x_send, x_recv,
 ):
     fs, tp = lax.axis_index("fs"), lax.axis_index("tp")
     z, y = lax.div(fs, R), lax.rem(fs, R)
@@ -202,9 +208,10 @@
     links = {(a, g): near(a, g) for a in "yz" for g in (1, -1)}
     right, left = near("x", 1), near("x", -1)
     partner = (fs, x * 2 + 1 - c)
+    across = [(fs, lax.rem(x + g, 4) * 2 + 1 - c) for g in (1, 3)]
 
     barrier = pltpu.get_barrier_semaphore()
-    peers = list(links.values()) + [right, left, partner]
+    peers = list(links.values()) + [right, left, partner] + across
     for peer in peers:
         pl.semaphore_signal(barrier, inc=1, device_id=peer, device_id_type=MESH)
 
@@ -327,6 +334,41 @@
             fbuf[i, side, :, 384:] = tail.astype(jnp.bfloat16)
             final_copy(i, side).start()
 
+    late = [arg for name, arg in steps if name == "L"]
+
+    def across_copy(i, side):
+        return pltpu.make_async_remote_copy(
+            src_ref=psend.at[i, lax.rem(x + 2, 4), :, pl.ds(side * 384, 384)], dst_ref=r2.at[late.index(i), side],
+            send_sem=x_send, recv_sem=x_recv.at[late.index(i), side],
+            device_id=across[side], device_id_type=MESH,
+        )
+
+    def step_l(i):
+        step_d(i)
+        total = pown[i, lax.rem(x + 2, 4)].astype(jnp.bfloat16)
+        sbuf[i, 0] = total[:, :384]
+        sbuf[i, 1] = total[:, 384:]
+        for side in (0, 1):
+            across_copy(i, side).start()
+            relay_copy(i, side).start()
+
+    def step_m(i):
+        pair_copy(i).wait_recv()
+        for side in (0, 1):
+            relay_copy(i, side).wait_recv()
+            across_copy(i, side).wait_recv()
+            own = summed(i, lax.rem(x + (1, 3)[side], 4))
+            extra = r1[i, side].astype(jnp.float32) + r2[late.index(i), side].astype(jnp.float32)
+            head, tail = own[:, :384], own[:, 384:]
+            if side == 0:
+                head = head + extra
+            else:
+                tail = tail + extra
+            fbuf[i, side, :, :384] = head.astype(jnp.bfloat16)
+            fbuf[i, side, :, 384:] = tail.astype(jnp.bfloat16)
+            final_copy(i, side).start()
+        pown[i, x] = summed(i, x)
+
     def step_g(i):
         total = pown[i, x]
         for side in (0, 1):
@@ -334,7 +376,7 @@
             total = total + gbuf[i, side].astype(jnp.float32)
         out_t[pl.ds(pl.multiple_of(row_in_block(i), ROWS), ROWS), :] = total
 
-    run = {"norm": norm, "U": up, "D": step_d, "E": step_e, "F": step_f, "G": step_g}
+    run = {"norm": norm, "U": up, "D": step_d, "E": step_e, "F": step_f, "G": step_g, "L": step_l, "M": step_m}
     for name, arg in steps:
         if name == "wait":
             copy_of(arg, False).wait_recv()
@@ -355,6 +397,7 @@
     sent(psend, d_send)
     sent(sbuf, s_send)
     sent(fbuf, f_send)
+    sent(r2, x_send)
 
 
 def scoped_kernel(msgs, steps, index, *refs):
@@ -362,7 +405,7 @@
     pl.run_scoped(
         functools.partial(kernel, msgs, steps, index, *refs),
         dma((6,)), dma((4,)), dma((len(msgs),)), dma, dma((16,)),
-        dma, dma((16, 2)), dma, dma((16, 2)),
+        dma, dma((16, 2)), dma, dma((16, 2)), dma, dma((LAST, 2)),
     )
 
 
@@ -391,6 +434,7 @@
             pltpu.VMEM((16, 4, 16, 768), f32),
             pltpu.VMEM((16, 2, 16, 384), bf16),
             pltpu.VMEM((16, 2, 16, 384), bf16),
+            pltpu.VMEM((LAST, 2, 16, 384), bf16),
             pltpu.VMEM((16, 2, 16, 768), bf16),
             pltpu.VMEM((16, 2, 16, 768), bf16),
             pltpu.VMEM((256, 768), f32),

time: 70.9 us -> 71.1 us (level)
  no operation moved by 1% of the time
where the time goes in v5:
time: 71.1 us; the launch traced here: 71 us
  Pallas kernels  70.2 us (99%)
  local copies, waits for them, and re-layouts  0.75 us (1%)
    pallas_call x1, Pallas kernels, on_device(): pl.pallas_call(functools.partial(scoped_kernel, msgs, steps, index), out_...  70.2 us

profile of v5, /device:TPU:1, one launch (start us, length us, event | category | flops | bytes accessed | tf_op | source)
XLA Modules:
  0.0 71.0 jit_solution(7091480606363411207)
XLA Ops:
  0.0 70.2 %shard_map.64 = bf16[768,256]{1,0:T(8,128)(2,1)S(1)} custom-call(bf16[768,2048]{1,0:T(8,128)(2,1)} %refs_0_.1, f32[1,2048]{1,0:T(1,128)} %bitcast.4, f32[32,1024]{1,0:T(8,128)} %refs_2_.1, f32[1,1024]{1,0:T(1,128)} %bitcast.5, f32[32,1024]{1,0:T(8,128)} %bitcast.3, f32[1,2048]{1,0:T(1,128)} %refs_5_.1), custom_call_target="tpu_custom_call" | custom-call | tf_op jit(solution)/shard_map/pallas_call | solution.py:416
  70.2 0.7 %copy.8 = bf16[768,256]{1,0:T(8,128)(2,1)} copy(bf16[768,256]{1,0:T(8,128)(2,1)S(1)} %shard_map.64) | data formatting | bytes 786432
